TPU v7x, 32 devices: a whole 2x2x4 slice. The times are simulated.
32 devices in a mesh: dp: 4 (over y, x), kv: 4 (over z), tp: 2 (over core).
Axes of the slice: x: 2, y: 2, z: 4, core: 2. Of those that a mesh axis runs over, the one named last changes fastest.
Arguments:
- tokens: bfloat16 [16, 16, 2048], P('dp', None, 'kv'), may hold values from -6 to 6
- norm_gain: float32 [2048], P('kv'), may hold values from 0.1 to 1.9
- w_query: bfloat16 [2048, 1024], P('kv', 'tp'), may hold values from -0.125 to 0.125
- w_key: bfloat16 [2048, 1024], P('kv', 'tp'), may hold values from -0.125 to 0.125
- w_value: bfloat16 [2048, 1024], P('kv', 'tp'), may hold values from -0.125 to 0.125
- w_forget: bfloat16 [2048, 16], replicated, may hold values from -0.125 to 0.125
- forget_bias: float32 [16], replicated, may hold values from -2 to 4
- query_gain: float32 [64], replicated, may hold values from 0.1 to 1.9
- key_gain: float32 [64], replicated, may hold values from 0.1 to 1.9
- head_gain: float32 [64], replicated, may hold values from 0.1 to 1.9
- w_out: bfloat16 [1024, 2048], P('tp', 'kv'), may hold values from -0.1875 to 0.1875
- key_cache: bfloat16 [16, 2048, 1024], P('dp', 'kv', 'tp'), may hold values from -240 to 240
- value_cache: bfloat16 [16, 2048, 1024], P('dp', 'kv', 'tp'), may hold values from -6 to 6
- gate_cache: float32 [16, 16, 2048], P('dp', 'tp', 'kv'), may hold values from -242 to 0, as said below
- lengths: int32 [16], P('dp'), may hold values from 1005 to 2028
- accepted: int32 [16], P('dp'), may hold values from 0 to 4
- parents: int32 [16, 16], P('dp'), may hold values from -1 to 14, as said below
Outputs:
- layer_out: bfloat16 [16, 16, 2048], P('dp', None, 'kv')
- new_keys: bfloat16 [16, 2048, 1024], P('dp', 'kv', 'tp')
- new_values: bfloat16 [16, 2048, 1024], P('dp', 'kv', 'tp')
- proposal_gates: float32 [16, 16, 16], P('dp', None, 'tp')
Inputs may be any that keep to these rules, and one draw needn't show every extreme that they name: `gate_cache`: each entry is the running sum of log forget gates up to its position, so entries never rise along positions; entries at and after lengths hold the last step's proposals in order. `parents`: proposal 0 follows the last accepted token (parent -1); every other proposal's parent is one of the three proposals before it.
All inputs are finite; a program needn't handle non-finite values.
Results may differ from a plain program's by a relative error of at most 0.0051.
The roundings to bfloat16 on the way count: a program that leaves them out, or rounds other values in their place, can miss the bound.
Values may be sent and summed in bfloat16 or wider, within the bound.
A program may use at most 64 MiB of HBM per device.

v0:
```python
import jax
import jax.numpy as jnp
from jax import lax
from jax.sharding import PartitionSpec as P

EPSILON = 1e-06
MASKED = -1e30


def head_norm(head_rows, gain_vec):
    mean_square = jnp.mean(head_rows * head_rows, axis=-1, keepdims=True)
    return head_rows * lax.rsqrt(mean_square + EPSILON) * gain_vec


def ancestry(parents):
    count_all = parents.shape[1]
    step_ids = jnp.arange(count_all, dtype=jnp.int32)
    step_matrix = (parents[:, :, None] == step_ids[None, None, :]).astype(jnp.float32)
    identity = jnp.broadcast_to(jnp.eye(count_all, dtype=jnp.float32), step_matrix.shape)

    def extend(turn_index, ancestors):
        return identity + jnp.einsum(
            "sij,sjk->sik", step_matrix, ancestors, precision=lax.Precision.HIGHEST
        )

    return lax.fori_loop(0, count_all, extend, identity)


def combine(earlier, later):
    earlier_max, earlier_total, earlier_sum = earlier
    later_max, later_total, later_sum = later
    row_max = jnp.maximum(earlier_max, later_max)
    earlier_scale = jnp.exp(earlier_max - row_max)
    later_scale = jnp.exp(later_max - row_max)
    spread = earlier_max.shape + (-1,)
    joined = (
        earlier_sum.reshape(spread) * earlier_scale[..., None]
        + later_sum.reshape(spread) * later_scale[..., None]
    )
    return (
        row_max,
        earlier_total * earlier_scale + later_total * later_scale,
        joined.reshape(earlier_sum.shape),
    )


def block_part(scores, live_mask, block_values):
    seq_count, heads_local, prop_count, key_count = scores.shape
    row_max = jnp.max(scores, axis=3)
    weights = jnp.where(live_mask, jnp.exp(scores - row_max[..., None]), 0.0)
    row_total = jnp.sum(weights, axis=3)
    weighted = jnp.einsum(
        "shpk,skhd->sphd",
        weights.astype(jnp.bfloat16),
        block_values,
        preferred_element_type=jnp.float32,
    )
    return (
        jnp.transpose(row_max, (0, 2, 1)),
        jnp.transpose(row_total, (0, 2, 1)),
        weighted.reshape(seq_count, prop_count, -1),
    )


def finish_rows(row_sums, inverse, query_gain, key_gain, heads_local):
    head_width = row_sums.shape[1] // 3
    head_size = head_width // heads_local
    row_count = row_sums.shape[0]
    raw_sums = row_sums * inverse[:, None]
    queries = head_norm(
        raw_sums[:, :head_width].reshape(row_count, heads_local, head_size), query_gain
    )
    keyed = head_norm(
        raw_sums[:, head_width : 2 * head_width].reshape(row_count, heads_local, head_size),
        key_gain,
    )
    return jnp.concatenate(
        [
            queries.reshape(row_count, head_width),
            keyed.reshape(row_count, head_width),
            raw_sums[:, 2 * head_width :],
        ],
        axis=1,
    ).astype(jnp.bfloat16)


def flatten_part(part_triple, rows_all):
    part_max, part_total, part_sum = part_triple
    return (
        part_max.reshape(rows_all, -1),
        part_total.reshape(rows_all, -1),
        part_sum.reshape(rows_all, -1),
    )


def shards(
    tokens,
    norm_gain,
    w_query,
    w_key,
    w_value,
    w_forget,
    forget_bias,
    query_gain,
    key_gain,
    head_gain,
    w_out,
    key_cache,
    value_cache,
    gate_cache,
    lengths,
    accepted,
    parents,
):
    seq_count, prop_count, width_in = tokens.shape
    pos_dev = key_cache.shape[1]
    heads_local = gate_cache.shape[1]
    head_width = key_cache.shape[2]
    head_size = head_width // heads_local
    rows_all = seq_count * prop_count
    full_width = w_forget.shape[0]
    kv_index = lax.axis_index("kv")
    tp_index = lax.axis_index("tp")
    flattened = tokens.reshape(rows_all, width_in).astype(jnp.float32)
    squares = jnp.sum(flattened * flattened, axis=1)
    scaled = (flattened * norm_gain).astype(jnp.bfloat16)
    w_rows = lax.dynamic_slice_in_dim(w_forget, kv_index * width_in, width_in, 0)
    gate_part = jnp.dot(scaled, w_rows, preferred_element_type=jnp.float32)
    w_joined = jnp.concatenate([w_query, w_key, w_value], axis=1)
    summed, gate_sum, square_sum = lax.psum(
        (jnp.dot(scaled, w_joined, preferred_element_type=jnp.float32), gate_part, squares), "kv"
    )
    inverse = lax.rsqrt(square_sum / full_width + EPSILON)
    joined = finish_rows(summed, inverse, query_gain, key_gain, heads_local)
    log_all = jax.nn.log_sigmoid(gate_sum * inverse[:, None] + forget_bias)
    log_own = lax.dynamic_slice_in_dim(log_all, tp_index * heads_local, heads_local, 1)
    log_own = log_own.reshape(seq_count, prop_count, heads_local)
    queries = joined[:, :head_width].reshape(seq_count, prop_count, heads_local, head_size)
    keys_new = joined[:, head_width : 2 * head_width].reshape(
        seq_count, prop_count, heads_local, head_size
    )
    values_new = joined[:, 2 * head_width :].reshape(seq_count, prop_count, heads_local, head_size)
    ancestors = ancestry(parents)
    path_sum = jnp.einsum("sij,sjh->sih", ancestors, log_own, precision=lax.Precision.HIGHEST)
    base_pos = lengths + accepted
    positions = kv_index * pos_dev + jnp.arange(pos_dev, dtype=jnp.int32)
    score_scale = head_size ** (-0.5)
    cached_keys = key_cache.reshape(seq_count, pos_dev, heads_local, head_size)
    cached_values = value_cache.reshape(seq_count, pos_dev, heads_local, head_size)
    scores = jnp.einsum("sphd,skhd->shpk", queries, cached_keys, preferred_element_type=jnp.float32)
    scores = scores * score_scale - gate_cache[:, :, None, :]
    live_mask = (positions[None, :] < base_pos[:, None])[:, None, None, :]
    scores = jnp.where(live_mask, scores, MASKED)
    local_part = block_part(scores, live_mask, cached_values)
    hit_mask = positions[None, :] == (base_pos - 1)[:, None]
    boundary_local = jnp.sum(jnp.where(hit_mask[:, None, :], gate_cache, 0.0), axis=2)
    tree_live = (ancestors > 0.5)[:, None, :, :]
    boundary = lax.psum(boundary_local, "kv")
    flat_max, flat_total, flat_sum = flatten_part(local_part, rows_all)
    got_max, got_total, got_sum = (
        lax.all_to_all(flat_max[None], "kv", split_axis=1, concat_axis=0, tiled=True),
        lax.all_to_all(flat_total[None], "kv", split_axis=1, concat_axis=0, tiled=True),
        lax.all_to_all(flat_sum[None], "kv", split_axis=1, concat_axis=0, tiled=True),
    )
    top = jnp.max(got_max, axis=0)
    factors = jnp.exp(got_max - top[None])
    own_rows = got_max.shape[1]
    summed_rows = jnp.sum(
        got_sum.reshape(got_sum.shape[0], own_rows, heads_local, head_size) * factors[..., None],
        axis=0,
    )
    merged = (top, jnp.sum(got_total * factors, axis=0), summed_rows.reshape(own_rows, head_width))
    tree_scores = jnp.einsum(
        "sphd,sjhd->shpj", queries, keys_new, preferred_element_type=jnp.float32
    )
    tree_scores = (
        tree_scores * score_scale
        - jnp.transpose(path_sum, (0, 2, 1))[:, :, None, :]
        - boundary[:, :, None, None]
    )
    tree_scores = jnp.where(tree_live, tree_scores, MASKED)
    tree_max, tree_total, tree_sum = flatten_part(
        block_part(tree_scores, tree_live, values_new), rows_all
    )
    row_lower = kv_index * own_rows
    merged = combine(
        merged,
        (
            lax.dynamic_slice_in_dim(tree_max, row_lower, own_rows, 0),
            lax.dynamic_slice_in_dim(tree_total, row_lower, own_rows, 0),
            lax.dynamic_slice_in_dim(tree_sum, row_lower, own_rows, 0),
        ),
    )
    row_max, row_total, weighted = merged
    attended = weighted.reshape(own_rows, heads_local, head_size) / row_total[..., None]
    own_normed = head_norm(attended, head_gain).astype(jnp.bfloat16).reshape(own_rows, head_width)
    normed = lax.all_gather(own_normed, "kv", axis=0, tiled=True)
    out_term = jnp.dot(normed, w_out, preferred_element_type=jnp.float32)
    layer_out = lax.psum(out_term.astype(jnp.bfloat16), "tp")
    layer_out = layer_out.reshape(seq_count, prop_count, -1)
    new_rows = jnp.concatenate(
        [
            keys_new.reshape(seq_count, prop_count, head_width),
            values_new.reshape(seq_count, prop_count, head_width),
        ],
        axis=2,
    )
    slot_index = positions[None, :, None] - base_pos[:, None, None]
    placing = slot_index == jnp.arange(prop_count, dtype=jnp.int32)[None, None, :]
    written = jnp.einsum(
        "skp,spc->skc", placing.astype(jnp.bfloat16), new_rows, preferred_element_type=jnp.float32
    ).astype(jnp.bfloat16)
    hit_rows = jnp.any(placing, axis=2)[..., None]
    new_keys = jnp.where(hit_rows, written[..., :head_width], key_cache)
    new_values = jnp.where(hit_rows, written[..., head_width:], value_cache)
    return (layer_out, new_keys, new_values, log_own)


def solution(mesh):
    placed = (
        P("dp", None, "kv"),
        P("kv"),
        P("kv", "tp"),
        P("kv", "tp"),
        P("kv", "tp"),
        P(),
        P(),
        P(),
        P(),
        P(),
        P("tp", "kv"),
        P("dp", "kv", "tp"),
        P("dp", "kv", "tp"),
        P("dp", "tp", "kv"),
        P("dp"),
        P("dp"),
        P("dp", None),
    )
    return jax.shard_map(
        shards,
        mesh=mesh,
        in_specs=placed,
        out_specs=(
            P("dp", None, "kv"),
            P("dp", "kv", "tp"),
            P("dp", "kv", "tp"),
            P("dp", None, "tp"),
        ),
        check_vma=False,
    )
```

profile of v0, /device:TPU:0, one launch (start us, length us, event | category | flops | bytes accessed | tf_op | source)
XLA Modules:
  0.0 129.3 jit_solution(6320880123169172122)
XLA Ops:
  7.2 0.9 fusion.29
  8.3 2.6 %fusion.6 = f32[64,1536]{1,0:T(8,128)} fusion(bf16[64,512]{1,0:T(8,128)(2,1)S(1)} %fusion.29, bf16[512,512]{1,0:T(8,128)(2,1)} %param.23, bf16[512,512]{1,0:T(8,128)(2,1)} %param.22, bf16[512,512]{1,0:T(8,128)(2,1)} %param.21), kind=kOutput, calls=%fused_computation.9 | convolution fusion | flops 105381888 | bytes 2031616 | tf_op jit(solution)/shard_map/dot_general | solution.py:131
  11.2 4.2 %while.11 = (s32[]{:T(128)}, f32[4,16,16]{2,1,0:T(8,128)S(1)}, s32[4,16]{1,0:T(4,128)S(1)}, f32[16,16]{1,0:T(8,128)S(1)}, s32[]{:T(128)}) while((s32[]{:T(128)}, f32[4,16,16]{2,1,0:T(8,128)S(1)}, s32[4,16]{1,0:T(4,128)S(1)}, f32[16,16]{1,0:T(8,128)S(1)}, s32[]{:T(128)}) %tuple.50), condition=%wide.region_8.9_spmd.clone, body=%wide.region_7.8_spmd.clone.sunk | while | flops 199682 | bytes 17725 | solution.py:26
  11.3 0.2 convolution_add_fusion.2
  11.5 0.2 convolution_add_fusion.2
  11.8 0.2 convolution_add_fusion.2
  12.1 0.2 convolution_add_fusion.2
  12.3 0.2 convolution_add_fusion.2
  12.6 0.2 convolution_add_fusion.2
  12.8 0.2 convolution_add_fusion.2
  13.1 0.2 convolution_add_fusion.2
  13.4 0.2 convolution_add_fusion.2
  13.6 0.2 convolution_add_fusion.2
  13.9 0.2 convolution_add_fusion.2
  14.2 0.2 convolution_add_fusion.2
  14.4 0.2 convolution_add_fusion.2
  14.7 0.2 convolution_add_fusion.2
  15.0 0.2 convolution_add_fusion.2
  15.6 0.8 fusion.39
  16.4 20.4 %all-reduce = (f32[64]{0:T(128)S(1)}, f32[4,8]{1,0:T(4,128)S(1)}, f32[64,16]{0,1:T(8,128)S(1)}) all-reduce(f32[64]{0:T(128)S(1)} %reduce_sum.86, f32[4,8]{1,0:T(4,128)S(1)} %select_reduce_fusion, f32[64,16]{0,1:T(8,128)S(1)} %fusion.39), channel_id=1, replica_groups=mesh['dp'=4,'kv'=4,'tp'=2] {'kv'}, use_global_device_ids=true, to_apply=%region_2.0 | all-reduce | flops 1120 | bytes 8960 | tf_op jit(solution)/shard_map/psum | solution.py:130
  37.4 4.3 %copy.136 = bf16[4,512,512]{1,2,0:T(8,128)(2,1)} copy(bf16[4,512,512]{2,1,0:T(8,128)(2,1)} %param.30) | data formatting | bytes 4194304 | tf_op args[11]
  41.7 2.4 %copy.138 = bf16[4,512,512]{1,2,0:T(8,128)(2,1)} copy(bf16[4,512,512]{2,1,0:T(8,128)(2,1)S(1)} %copy-done.1) | data formatting | bytes 4194304 | tf_op args[12]
  44.3 6.7 %all-reduce.4.cloned.1.call-done = f32[64,1536]{1,0:T(8,128)} async-done(((f32[64,1536]{1,0:T(8,128)}), f32[64,1536]{1,0:T(8,128)}) %all-reduce.4.cloned.1.call-update) | async-done | bytes 393232 | tf_op jit(solution)/shard_map/psum | solution.py:130
  51.0 1.1 broadcast_multiply_fusion
  53.9 2.1 %fusion.57 = (f32[4,8,16]{2,1,0:T(8,128)S(1)}, f32[4,8,16,512]{3,2,1,0:T(8,128)S(1)}) fusion(f32[4,8,512]{2,1,0:T(8,128)S(1)} %copy-done.3, bf16[4,512,8,64]{1,3,2,0:T(8,128)(2,1)} %bitcast.48, bf16[4,16,8,64]{3,2,1,0:T(8,128)(2,1)S(1)} %reshape.230, pred[4,512]{1,0:T(4,128)(4,1)S(1)} %get-tuple-element.90), kind=kOutput, calls=%fused_computation.96 | convolution fusion | flops 34602496 | bytes 3280896 | tf_op jit(solution)/shard_map/sphd,skhd->shpk/dot_general | solution.py:150
  56.0 0.3 fusion.17
  56.4 0.5 broadcast.155
  57.0 0.7 reduce.2
  57.7 0.7 reshape.243
  58.3 3.4 %all-to-all-start.2 = ((f32[4,1,128]{2,1,0:T(1,128)}), f32[4,1,128]{2,1,0:T(1,128)S(1)}, u32[]{:S(2)}, u32[]{:S(2)}) async-start(f32[4,1,128]{2,1,0:T(1,128)} %reshape.243), calls=%async_computation.2 | async-start | bytes 4096 | tf_op jit(solution)/shard_map/all_to_all | solution.py:162
  61.8 2.3 %convolution_bitcast_fusion = f32[4,16,8,64]{3,1,2,0:T(8,128)S(1)} fusion(bf16[4,512,8,64]{1,3,2,0:T(8,128)(2,1)} %bitcast.47, f32[4,8,16,512]{3,2,1,0:T(8,128)S(1)} %get-tuple-element.95, f32[4,8,16]{2,1,0:T(8,128)S(1)} %get-tuple-element.94, pred[4,512]{1,0:T(4,128)(4,1)S(1)} %get-tuple-element.90), kind=kOutput, calls=%fused_computation.21 | convolution fusion | flops 34340864 | bytes 3280896 | tf_op jit(solution)/shard_map/shpk,skhd->sphd/dot_general | solution.py:52
  64.1 3.2 %convolution_convert_fusion = bf16[4,512,1024]{2,1,0:T(8,128)(2,1)} fusion(bf16[4,16,512]{2,1,0:T(8,128)(2,1)S(1)} %bitcast.50, bf16[4,16,512]{2,1,0:T(8,128)(2,1)S(1)} %bitcast.49, s32[4,512]{1,0:T(4,128)S(1)} %broadcast_subtract_fusion), kind=kOutput, calls=%fused_computation.6 | convolution fusion | flops 69500928 | bytes 4333568 | tf_op jit(solution)/shard_map/skp,spc->skc/dot_general | solution.py:210
  67.3 0.2 fusion.56
  67.6 0.2 convolution_bitcast_fusion.1
  68.2 0.7 reduce.4
  68.9 0.7 reshape.241
  69.6 5.1 %all-to-all-start.1 = ((f32[4,1,128]{2,1,0:T(1,128)}), f32[4,1,128]{2,1,0:T(1,128)S(1)}, u32[]{:S(2)}, u32[]{:S(2)}) async-start(f32[4,1,128]{2,1,0:T(1,128)} %reshape.241), calls=%async_computation.1 | async-start | bytes 4096 | tf_op jit(solution)/shard_map/all_to_all | solution.py:161
  75.0 0.8 broadcast_in_dim_reshape_reshape.4
  75.8 0.6 reduce.3
  76.6 3.6 %all-to-all-done.1 = f32[4,1,128]{2,1,0:T(1,128)S(1)} async-done(((f32[4,1,128]{2,1,0:T(1,128)}), f32[4,1,128]{2,1,0:T(1,128)S(1)}, u32[]{:S(2)}, u32[]{:S(2)}) %all-to-all-start.1) | async-done | bytes 2080 | tf_op jit(solution)/shard_map/all_to_all | solution.py:161
  80.1 3.3 %all-to-all-start = ((f32[1,64,512]{2,0,1:T(1,128)}), f32[1,64,512]{2,0,1:T(1,128)S(1)}, u32[]{:S(2)}, u32[]{:S(2)}) async-start(f32[1,64,512]{2,0,1:T(1,128)} %broadcast_in_dim_reshape_reshape.4), calls=%async_computation | async-start | bytes 262144 | tf_op jit(solution)/shard_map/all_to_all | solution.py:163
  83.5 0.6 reduce.5
  85.2 4.2 %all-to-all-done = f32[1,64,512]{2,0,1:T(1,128)S(1)} async-done(((f32[1,64,512]{2,0,1:T(1,128)}), f32[1,64,512]{2,0,1:T(1,128)S(1)}, u32[]{:S(2)}, u32[]{:S(2)}) %all-to-all-start) | async-done | bytes 131104 | tf_op jit(solution)/shard_map/all_to_all | solution.py:163
  90.1 13.1 %all_gather.3 = bf16[64,512]{1,0:T(8,128)(2,1)S(1)} all-gather(bf16[16,512]{1,0:T(8,128)(2,1)S(1)} %multiply_convert_fusion.2), channel_id=1, replica_groups=mesh['dp'=4,'kv'=4,'tp'=2] {'kv'}, dimensions={0}, use_global_device_ids=true | all-gather | bytes 81920 | tf_op jit(solution)/shard_map/all_gather | solution.py:197
  103.2 0.8 convolution_convert_fusion.1
  104.1 4.4 %slice_select_fusion = (bf16[4,512,512]{2,1,0:T(8,128)(2,1)}, bf16[4,512,512]{2,1,0:T(8,128)(2,1)}) fusion(bf16[4,512,512]{2,1,0:T(8,128)(2,1)S(1)} %copy-done.2, bf16[4,512,1024]{2,1,0:T(8,128)(2,1)} %convolution_convert_fusion, pred[4,512]{1,0:T(4,128)(4,1)S(1)} %fusion.32, bf16[4,512,512]{2,1,0:T(8,128)(2,1)} %param.30), kind=kLoop, calls=%fused_computation.7 | loop fusion | flops 2097152 | bytes 12584960 | tf_op jit(solution)/shard_map/jit(_where)/select_n | solution.py:215
  108.5 12.4 %all-reduce.6.cloned.1.call-done = bf16[4,16,512]{2,1,0:T(8,128)(2,1)} async-done(((bf16[4,16,512]{2,1,0:T(8,128)(2,1)}), bf16[4,16,512]{2,1,0:T(8,128)(2,1)}) %all-reduce.6.cloned.1.call-update) | async-done | bytes 65552 | tf_op jit(solution)/shard_map/psum | solution.py:199
  121.0 1.5 %copy.192 = bf16[4,16,512]{2,1,0:T(8,128)(2,1)} copy(bf16[4,16,512]{2,1,0:T(8,128)(2,1)} %all-reduce.6.cloned.1.call-done) | data formatting | bytes 131072
  (122 shorter events, 5.9 us)
Async XLA Ops:
  7.2 96.0 %copy-start = (bf16[512,512]{1,0:T(8,128)(2,1)S(1)}, bf16[512,512]{1,0:T(8,128)(2,1)}, u32[]{:S(2)}) copy-start(bf16[512,512]{1,0:T(8,128)(2,1)} %param.29) | copy-start | bytes 1572868
  7.2 43.8 %all-reduce.4.cloned.1.call-start = ((), (), s32[]{:S(2)}) async-start(), calls=%async_computation.3 | async-start | bytes 786432 | tf_op jit(solution)/shard_map/psum | solution.py:130
  8.1 2.7 %copy-start.4 = (bf16[4,16,512]{2,1,0:T(8,128)(2,1)S(1)}, bf16[4,16,512]{2,1,0:T(8,128)(2,1)}, u32[]{:S(2)}) copy-start(bf16[4,16,512]{2,1,0:T(8,128)(2,1)} %param.19) | copy-start | bytes 196612
  8.2 2.9 %copy-start.11 = (s32[4]{0:T(128)S(1)}, s32[4]{0:T(128)}, u32[]{:S(2)}) copy-start(s32[4]{0:T(128)} %param.33) | copy-start | bytes 52
  8.2 2.9 %copy-start.12 = (s32[4]{0:T(128)S(1)}, s32[4]{0:T(128)}, u32[]{:S(2)}) copy-start(s32[4]{0:T(128)} %param.34) | copy-start | bytes 52
  8.2 3.0 %copy-start.6 = (s32[4,16]{1,0:T(4,128)S(1)}, s32[4,16]{1,0:T(4,128)}, u32[]{:S(2)}) copy-start(s32[4,16]{1,0:T(4,128)} %param.35) | copy-start | bytes 772
  8.2 7.3 %copy-start.3 = (f32[4,8,512]{2,1,0:T(8,128)S(1)}, f32[4,8,512]{2,1,0:T(8,128)}, u32[]{:S(2)}) copy-start(f32[4,8,512]{2,1,0:T(8,128)} %param.32) | copy-start | bytes 196612
  8.2 28.7 %copy-start.7 = (f32[16]{0:T(128)S(1)}, f32[16]{0:T(128)}, u32[]{:S(2)}) copy-start(f32[16]{0:T(128)} %param.25) | copy-start | bytes 196
  8.2 28.8 %copy-start.8 = (f32[64]{0:T(128)S(1)}, f32[64]{0:T(128)}, u32[]{:S(2)}) copy-start(f32[64]{0:T(128)} %param.26) | copy-start | bytes 772
  8.2 28.8 %copy-start.9 = (f32[64]{0:T(128)S(1)}, f32[64]{0:T(128)}, u32[]{:S(2)}) copy-start(f32[64]{0:T(128)} %param.27) | copy-start | bytes 772
  8.2 28.9 %copy-start.10 = (f32[64]{0:T(128)S(1)}, f32[64]{0:T(128)}, u32[]{:S(2)}) copy-start(f32[64]{0:T(128)} %param.28) | copy-start | bytes 772
  37.4 6.7 %copy-start.5 = (f32[4,16,8]{1,2,0:T(8,128)}, f32[4,16,8]{1,2,0:T(8,128)S(1)}, u32[]{:S(2)}) copy-start(f32[4,16,8]{1,2,0:T(8,128)S(1)} %copy.148) | copy-start | bytes 6148
  37.4 4.3 %copy-start.1 = (bf16[4,512,512]{2,1,0:T(8,128)(2,1)S(1)}, bf16[4,512,512]{2,1,0:T(8,128)(2,1)}, u32[]{:S(2)}) copy-start(bf16[4,512,512]{2,1,0:T(8,128)(2,1)} %param.31) | copy-start | bytes 6291460
  58.3 11.2 %all-to-all-start.2 = ((f32[4,1,128]{2,1,0:T(1,128)}), f32[4,1,128]{2,1,0:T(1,128)S(1)}, u32[]{:S(2)}, u32[]{:S(2)}) async-start(f32[4,1,128]{2,1,0:T(1,128)} %reshape.243), calls=%async_computation.2 | async-start | bytes 4096 | tf_op jit(solution)/shard_map/all_to_all | solution.py:162
  69.6 10.6 %all-to-all-start.1 = ((f32[4,1,128]{2,1,0:T(1,128)}), f32[4,1,128]{2,1,0:T(1,128)S(1)}, u32[]{:S(2)}, u32[]{:S(2)}) async-start(f32[4,1,128]{2,1,0:T(1,128)} %reshape.241), calls=%async_computation.1 | async-start | bytes 4096 | tf_op jit(solution)/shard_map/all_to_all | solution.py:161
  75.0 29.1 %copy-start.2 = (bf16[4,512,512]{2,1,0:T(8,128)(2,1)S(1)}, bf16[4,512,512]{2,1,0:T(8,128)(2,1)}, u32[]{:S(2)}) copy-start(bf16[4,512,512]{2,1,0:T(8,128)(2,1)} %param.31) | copy-start | bytes 6291460
  80.1 9.2 %all-to-all-start = ((f32[1,64,512]{2,0,1:T(1,128)}), f32[1,64,512]{2,0,1:T(1,128)S(1)}, u32[]{:S(2)}, u32[]{:S(2)}) async-start(f32[1,64,512]{2,0,1:T(1,128)} %broadcast_in_dim_reshape_reshape.4), calls=%async_computation | async-start | bytes 262144 | tf_op jit(solution)/shard_map/all_to_all | solution.py:163
  83.5 37.5 %all-reduce.6.cloned.1.call-start = ((), (), s32[]{:S(2)}) async-start(), calls=%async_computation.4 | async-start | bytes 131072 | tf_op jit(solution)/shard_map/psum | solution.py:199
Sparse Core Ops, SparseCore 0:
  11.0 39.9 all-reduce.3
  104.2 16.7 all-reduce.5
where the time goes:
time: 130 us; the launch traced here: 129 us
  blocking collectives  33.6 us (26%)
  waiting for transfers between devices  27 us (21%)
  matrix products  16.2 us (12%)
  local copies, waits for them, and re-layouts  14.8 us (11%)
  between operations  14.5 us (11%)
  starting transfers between devices  11.9 us (9%)
  other arithmetic  10.9 us (8%)
    psum x1, blocking collectives, shards(): lax.psum((jnp.dot(scaled, w_joined, preferred_element_type=jnp.float32),...  20.4 us
    all_gather x1, blocking collectives, shards(): normed = lax.all_gather(own_normed, 'kv', axis=0, tiled=True)  13.1 us
    psum x1, waiting for transfers between devices, shards(): layer_out = lax.psum(out_term.astype(jnp.bfloat16), 'tp')  12.4 us
    unnamed x34, local copies, waits for them, and re-layouts  10.3 us
    psum x1, waiting for transfers between devices, shards(): lax.psum((jnp.dot(scaled, w_joined, preferred_element_type=jnp.float32),...  6.72 us
    all_to_all x1, starting transfers between devices, shards(): lax.all_to_all(flat_max[None], 'kv', split_axis=1, concat_axis=0, tiled=T...  5.09 us
    select_n x1, other arithmetic, shards(): new_values = jnp.where(hit_rows, written[..., head_width:], value_cache)  4.45 us
    all_to_all x1, waiting for transfers between devices, shards(): lax.all_to_all(flat_sum[None], 'kv', split_axis=1, concat_axis=0, tiled=T...  4.2 us
  transfers between devices with their start and end apart: 5, of which 4 were waited for; matrix products, arithmetic and copies ran while one was open for 22% of the time, Pallas kernels for 0%

commit v1 on v0

--- a/solution.py
+++ b/solution.py
@@ -5,6 +5,11 @@
 
 EPSILON = 1e-06
 MASKED = -1e30
+
+
+def supply_all_the_goods(slab_in, named_axis):
+    row_out = lax.all_gather(slab_in, named_axis)
+    return jnp.sum(row_out, 0)
 
 
 def head_norm(head_rows, gain_vec):
@@ -196,7 +201,7 @@
     own_normed = head_norm(attended, head_gain).astype(jnp.bfloat16).reshape(own_rows, head_width)
     normed = lax.all_gather(own_normed, "kv", axis=0, tiled=True)
     out_term = jnp.dot(normed, w_out, preferred_element_type=jnp.float32)
-    layer_out = lax.psum(out_term.astype(jnp.bfloat16), "tp")
+    layer_out = supply_all_the_goods(out_term.astype(jnp.bfloat16), "tp")
     layer_out = layer_out.reshape(seq_count, prop_count, -1)
     new_rows = jnp.concatenate(
         [

time: 130 us -> 115 us (0.88)
  waiting for transfers between devices: 27 us -> 14.5 us
  matrix products: 16.2 us -> 13.6 us
  blocking collectives: 33.6 us -> 35.5 us
    psum x1 -> x0, waiting for transfers between devices: 12.4 us -> none  [shards(): layer_out = lax.psum(out_term.astype(jnp.bfloat16), 'tp')]
    select_n x1, other arithmetic: 4.45 us -> 2.33 us  [shards(): new_values = jnp.where(hit_rows, written[..., head_width:], value_cache)]
    dot_general x1, matrix products: 3.24 us -> 1.31 us  [shards(): jnp.einsum('skp,spc->skc', placing.astype(jnp.bfloat16), new_rows, prefer...]
    all_gather x0 -> x1, blocking collectives: none -> 1.9 us  [supply_all_the_goods(): row_out = lax.all_gather(slab_in, named_axis)]
    unnamed x34 -> x35, local copies, waits for them, and re-layouts: 10.3 us -> 9.8 us
  transfers between devices with their start and end apart: 5 -> 4, of which waited for: 4 -> 3; matrix products, arithmetic and copies ran while one was open for 22% -> 21% of each run, Pallas kernels for 0% -> 0%
where the time goes in v1:
time: 115 us; the launch traced here: 114 us
  blocking collectives  35.5 us (31%)
  waiting for transfers between devices  14.5 us (13%)
  between operations  14.5 us (13%)
  local copies, waits for them, and re-layouts  14.3 us (12%)
  matrix products  13.6 us (12%)
  starting transfers between devices  11.9 us (10%)
  other arithmetic  9.68 us (8%)
    psum x1, blocking collectives, shards(): lax.psum((jnp.dot(scaled, w_joined, preferred_element_type=jnp.float32),...  20.4 us
    all_gather x1, blocking collectives, shards(): normed = lax.all_gather(own_normed, 'kv', axis=0, tiled=True)  13.1 us
    unnamed x35, local copies, waits for them, and re-layouts  9.8 us
    psum x1, waiting for transfers between devices, shards(): lax.psum((jnp.dot(scaled, w_joined, preferred_element_type=jnp.float32),...  6.72 us
    all_to_all x1, starting transfers between devices, shards(): lax.all_to_all(flat_max[None], 'kv', split_axis=1, concat_axis=0, tiled=T...  5.09 us
    all_to_all x1, waiting for transfers between devices, shards(): lax.all_to_all(flat_sum[None], 'kv', split_axis=1, concat_axis=0, tiled=T...  4.19 us
    dot_general x16, matrix products, extend(): jnp.einsum('sij,sjk->sik', step_matrix, ancestors, precision=lax.Precisio...  3.67 us
    all_to_all x1, waiting for transfers between devices, shards(): lax.all_to_all(flat_max[None], 'kv', split_axis=1, concat_axis=0, tiled=T...  3.62 us
  transfers between devices with their start and end apart: 4, of which 3 were waited for; matrix products, arithmetic and copies ran while one was open for 21% of the time, Pallas kernels for 0%

profile of v1, /device:TPU:0, one launch (start us, length us, event | category | flops | bytes accessed | tf_op | source)
XLA Modules:
  0.0 114.4 jit_solution(15848074861492798127)
XLA Ops:
  7.2 0.9 fusion.29
  8.3 2.6 %fusion.6 = f32[64,1536]{1,0:T(8,128)} fusion(bf16[64,512]{1,0:T(8,128)(2,1)S(1)} %fusion.29, bf16[512,512]{1,0:T(8,128)(2,1)} %param.23, bf16[512,512]{1,0:T(8,128)(2,1)} %param.22, bf16[512,512]{1,0:T(8,128)(2,1)} %param.21), kind=kOutput, calls=%fused_computation.9 | convolution fusion | flops 105381888 | bytes 2031616 | tf_op jit(solution)/shard_map/dot_general | solution.py:136
  11.2 4.2 %while.11 = (s32[]{:T(128)}, f32[4,16,16]{2,1,0:T(8,128)S(1)}, s32[4,16]{1,0:T(4,128)S(1)}, f32[16,16]{1,0:T(8,128)S(1)}, s32[]{:T(128)}) while((s32[]{:T(128)}, f32[4,16,16]{2,1,0:T(8,128)S(1)}, s32[4,16]{1,0:T(4,128)S(1)}, f32[16,16]{1,0:T(8,128)S(1)}, s32[]{:T(128)}) %tuple.47), condition=%wide.region_8.9_spmd.clone, body=%wide.region_7.8_spmd.clone.sunk | while | flops 199682 | bytes 17725 | solution.py:31
  11.3 0.2 convolution_add_fusion.2
  11.5 0.2 convolution_add_fusion.2
  11.8 0.2 convolution_add_fusion.2
  12.1 0.2 convolution_add_fusion.2
  12.3 0.2 convolution_add_fusion.2
  12.6 0.2 convolution_add_fusion.2
  12.8 0.2 convolution_add_fusion.2
  13.1 0.2 convolution_add_fusion.2
  13.4 0.2 convolution_add_fusion.2
  13.6 0.2 convolution_add_fusion.2
  13.9 0.2 convolution_add_fusion.2
  14.2 0.2 convolution_add_fusion.2
  14.7 0.2 convolution_add_fusion.2
  15.0 0.2 convolution_add_fusion.2
  15.6 0.8 fusion.39
  16.4 20.4 %all-reduce = (f32[64]{0:T(128)S(1)}, f32[4,8]{1,0:T(4,128)S(1)}, f32[64,16]{0,1:T(8,128)S(1)}) all-reduce(f32[64]{0:T(128)S(1)} %reduce_sum.98, f32[4,8]{1,0:T(4,128)S(1)} %select_reduce_fusion, f32[64,16]{0,1:T(8,128)S(1)} %fusion.39), channel_id=1, replica_groups=mesh['dp'=4,'kv'=4,'tp'=2] {'kv'}, use_global_device_ids=true, to_apply=%region_2.0 | all-reduce | flops 1120 | bytes 8960 | tf_op jit(solution)/shard_map/psum | solution.py:135
  37.4 4.3 %copy.136 = bf16[4,512,512]{1,2,0:T(8,128)(2,1)} copy(bf16[4,512,512]{2,1,0:T(8,128)(2,1)} %param.30) | data formatting | bytes 4194304 | tf_op args[11]
  41.7 2.4 %copy.138 = bf16[4,512,512]{1,2,0:T(8,128)(2,1)} copy(bf16[4,512,512]{2,1,0:T(8,128)(2,1)S(1)} %copy-done.1) | data formatting | bytes 4194304 | tf_op args[12]
  44.3 6.7 %all-reduce.3.cloned.1.call-done = f32[64,1536]{1,0:T(8,128)} async-done(((f32[64,1536]{1,0:T(8,128)}), f32[64,1536]{1,0:T(8,128)}) %all-reduce.3.cloned.1.call-update) | async-done | bytes 393232 | tf_op jit(solution)/shard_map/psum | solution.py:135
  51.0 1.1 broadcast_multiply_fusion
  53.9 2.1 %fusion.57 = (f32[4,8,16]{2,1,0:T(8,128)S(1)}, f32[4,8,16,512]{3,2,1,0:T(8,128)S(1)}) fusion(f32[4,8,512]{2,1,0:T(8,128)S(1)} %copy-done.4, bf16[4,512,8,64]{1,3,2,0:T(8,128)(2,1)} %bitcast.49, bf16[4,16,8,64]{3,2,1,0:T(8,128)(2,1)S(1)} %reshape.230, pred[4,512]{1,0:T(4,128)(4,1)S(1)} %get-tuple-element.90), kind=kOutput, calls=%fused_computation.96 | convolution fusion | flops 34602496 | bytes 3280896 | tf_op jit(solution)/shard_map/sphd,skhd->shpk/dot_general | solution.py:155
  56.0 0.3 fusion.17
  56.4 0.6 broadcast.155
  57.0 0.8 reduce.3
  57.8 0.7 reshape.244
  58.5 3.4 %all-to-all-start.2 = ((f32[4,1,128]{2,1,0:T(1,128)}), f32[4,1,128]{2,1,0:T(1,128)S(1)}, u32[]{:S(2)}, u32[]{:S(2)}) async-start(f32[4,1,128]{2,1,0:T(1,128)} %reshape.244), calls=%async_computation.2 | async-start | bytes 4096 | tf_op jit(solution)/shard_map/all_to_all | solution.py:167
  61.9 2.3 %convolution_bitcast_fusion = f32[4,16,8,64]{3,1,2,0:T(8,128)S(1)} fusion(bf16[4,512,8,64]{1,3,2,0:T(8,128)(2,1)} %bitcast.48, f32[4,8,16,512]{3,2,1,0:T(8,128)S(1)} %get-tuple-element.95, f32[4,8,16]{2,1,0:T(8,128)S(1)} %get-tuple-element.94, pred[4,512]{1,0:T(4,128)(4,1)S(1)} %get-tuple-element.90), kind=kOutput, calls=%fused_computation.21 | convolution fusion | flops 34340864 | bytes 3280896 | tf_op jit(solution)/shard_map/shpk,skhd->sphd/dot_general | solution.py:57
  64.2 1.3 %convolution_convert_fusion = bf16[4,512,1024]{2,1,0:T(8,128)(2,1)S(1)} fusion(bf16[4,16,512]{2,1,0:T(8,128)(2,1)S(1)} %bitcast.51, bf16[4,16,512]{2,1,0:T(8,128)(2,1)S(1)} %bitcast.50, s32[4,512]{1,0:T(4,128)S(1)} %broadcast_subtract_fusion), kind=kOutput, calls=%fused_computation.6 | convolution fusion | flops 69500928 | bytes 4333568 | tf_op jit(solution)/shard_map/skp,spc->skc/dot_general | solution.py:215
  65.5 0.3 copy-done.2
  65.8 0.6 copy-done.3
  66.4 2.3 %slice_select_fusion = (bf16[4,512,512]{2,1,0:T(8,128)(2,1)}, bf16[4,512,512]{2,1,0:T(8,128)(2,1)}) fusion(bf16[4,512,512]{2,1,0:T(8,128)(2,1)S(1)} %copy-done.2, bf16[4,512,1024]{2,1,0:T(8,128)(2,1)S(1)} %convolution_convert_fusion, pred[4,512]{1,0:T(4,128)(4,1)S(1)} %fusion.32, bf16[4,512,512]{2,1,0:T(8,128)(2,1)S(1)} %copy-done.3), kind=kLoop, calls=%fused_computation.7 | loop fusion | flops 2097152 | bytes 12584960 | tf_op jit(solution)/shard_map/jit(_where)/select_n | solution.py:220
  68.8 0.2 fusion.56
  69.0 0.2 convolution_bitcast_fusion.1
  69.6 0.8 reduce.5
  70.4 0.7 reshape.242
  71.1 5.1 %all-to-all-start.1 = ((f32[4,1,128]{2,1,0:T(1,128)}), f32[4,1,128]{2,1,0:T(1,128)S(1)}, u32[]{:S(2)}, u32[]{:S(2)}) async-start(f32[4,1,128]{2,1,0:T(1,128)} %reshape.242), calls=%async_computation.1 | async-start | bytes 4096 | tf_op jit(solution)/shard_map/all_to_all | solution.py:166
  76.5 0.8 broadcast_in_dim_reshape_reshape.4
  77.3 0.7 reduce.4
  78.1 3.6 %all-to-all-done.1 = f32[4,1,128]{2,1,0:T(1,128)S(1)} async-done(((f32[4,1,128]{2,1,0:T(1,128)}), f32[4,1,128]{2,1,0:T(1,128)S(1)}, u32[]{:S(2)}, u32[]{:S(2)}) %all-to-all-start.1) | async-done | bytes 2080 | tf_op jit(solution)/shard_map/all_to_all | solution.py:166
  81.7 3.3 %all-to-all-start = ((f32[1,64,512]{2,0,1:T(1,128)}), f32[1,64,512]{2,0,1:T(1,128)S(1)}, u32[]{:S(2)}, u32[]{:S(2)}) async-start(f32[1,64,512]{2,0,1:T(1,128)} %broadcast_in_dim_reshape_reshape.4), calls=%async_computation | async-start | bytes 262144 | tf_op jit(solution)/shard_map/all_to_all | solution.py:168
  85.1 0.7 reduce.6
  86.8 4.2 %all-to-all-done = f32[1,64,512]{2,0,1:T(1,128)S(1)} async-done(((f32[1,64,512]{2,0,1:T(1,128)}), f32[1,64,512]{2,0,1:T(1,128)S(1)}, u32[]{:S(2)}, u32[]{:S(2)}) %all-to-all-start) | async-done | bytes 131104 | tf_op jit(solution)/shard_map/all_to_all | solution.py:168
  91.6 13.1 %all_gather.9 = bf16[64,512]{1,0:T(8,128)(2,1)S(1)} all-gather(bf16[16,512]{1,0:T(8,128)(2,1)S(1)} %multiply_convert_fusion.2), channel_id=1, replica_groups=mesh['dp'=4,'kv'=4,'tp'=2] {'kv'}, dimensions={0}, use_global_device_ids=true | all-gather | bytes 81920 | tf_op jit(solution)/shard_map/all_gather | solution.py:202
  105.0 1.9 %all-gather = bf16[128,512]{1,0:T(8,128)(2,1)S(1)} all-gather(bf16[64,512]{1,0:T(8,128)(2,1)S(1)} %convolution_convert_fusion.1), channel_id=2, replica_groups=mesh['dp'=4,'kv'=4,'tp'=2] {'tp'}, dimensions={0}, use_global_device_ids=true | all-gather | bytes 196608 | tf_op jit(solution)/shard_map/all_gather | solution.py:11
  106.9 0.7 reduce_sum.108
  (122 shorter events, 6.3 us)
Async XLA Ops:
  7.2 97.6 %copy-start = (bf16[512,512]{1,0:T(8,128)(2,1)S(1)}, bf16[512,512]{1,0:T(8,128)(2,1)}, u32[]{:S(2)}) copy-start(bf16[512,512]{1,0:T(8,128)(2,1)} %param.29) | copy-start | bytes 1572868
  7.2 43.8 %all-reduce.3.cloned.1.call-start = ((), (), s32[]{:S(2)}) async-start(), calls=%async_computation.3 | async-start | bytes 786432 | tf_op jit(solution)/shard_map/psum | solution.py:135
  8.1 2.7 %copy-start.5 = (bf16[4,16,512]{2,1,0:T(8,128)(2,1)S(1)}, bf16[4,16,512]{2,1,0:T(8,128)(2,1)}, u32[]{:S(2)}) copy-start(bf16[4,16,512]{2,1,0:T(8,128)(2,1)} %param.19) | copy-start | bytes 196612
  8.2 2.9 %copy-start.12 = (s32[4]{0:T(128)S(1)}, s32[4]{0:T(128)}, u32[]{:S(2)}) copy-start(s32[4]{0:T(128)} %param.33) | copy-start | bytes 52
  8.2 2.9 %copy-start.13 = (s32[4]{0:T(128)S(1)}, s32[4]{0:T(128)}, u32[]{:S(2)}) copy-start(s32[4]{0:T(128)} %param.34) | copy-start | bytes 52
  8.2 3.0 %copy-start.7 = (s32[4,16]{1,0:T(4,128)S(1)}, s32[4,16]{1,0:T(4,128)}, u32[]{:S(2)}) copy-start(s32[4,16]{1,0:T(4,128)} %param.35) | copy-start | bytes 772
  8.2 7.3 %copy-start.4 = (f32[4,8,512]{2,1,0:T(8,128)S(1)}, f32[4,8,512]{2,1,0:T(8,128)}, u32[]{:S(2)}) copy-start(f32[4,8,512]{2,1,0:T(8,128)} %param.32) | copy-start | bytes 196612
  8.2 28.7 %copy-start.8 = (f32[16]{0:T(128)S(1)}, f32[16]{0:T(128)}, u32[]{:S(2)}) copy-start(f32[16]{0:T(128)} %param.25) | copy-start | bytes 196
  8.2 28.8 %copy-start.9 = (f32[64]{0:T(128)S(1)}, f32[64]{0:T(128)}, u32[]{:S(2)}) copy-start(f32[64]{0:T(128)} %param.26) | copy-start | bytes 772
  8.2 28.8 %copy-start.10 = (f32[64]{0:T(128)S(1)}, f32[64]{0:T(128)}, u32[]{:S(2)}) copy-start(f32[64]{0:T(128)} %param.27) | copy-start | bytes 772
  8.2 28.9 %copy-start.11 = (f32[64]{0:T(128)S(1)}, f32[64]{0:T(128)}, u32[]{:S(2)}) copy-start(f32[64]{0:T(128)} %param.28) | copy-start | bytes 772
  37.4 6.7 %copy-start.6 = (f32[4,16,8]{1,2,0:T(8,128)}, f32[4,16,8]{1,2,0:T(8,128)S(1)}, u32[]{:S(2)}) copy-start(f32[4,16,8]{1,2,0:T(8,128)S(1)} %copy.148) | copy-start | bytes 6148
  37.4 4.3 %copy-start.1 = (bf16[4,512,512]{2,1,0:T(8,128)(2,1)S(1)}, bf16[4,512,512]{2,1,0:T(8,128)(2,1)}, u32[]{:S(2)}) copy-start(bf16[4,512,512]{2,1,0:T(8,128)(2,1)} %param.31) | copy-start | bytes 6291460
  58.5 12.6 %all-to-all-start.2 = ((f32[4,1,128]{2,1,0:T(1,128)}), f32[4,1,128]{2,1,0:T(1,128)S(1)}, u32[]{:S(2)}, u32[]{:S(2)}) async-start(f32[4,1,128]{2,1,0:T(1,128)} %reshape.244), calls=%async_computation.2 | async-start | bytes 4096 | tf_op jit(solution)/shard_map/all_to_all | solution.py:167
  64.2 1.6 %copy-start.2 = (bf16[4,512,512]{2,1,0:T(8,128)(2,1)S(1)}, bf16[4,512,512]{2,1,0:T(8,128)(2,1)}, u32[]{:S(2)}) copy-start(bf16[4,512,512]{2,1,0:T(8,128)(2,1)} %param.31) | copy-start | bytes 6291460
  64.2 2.2 %copy-start.3 = (bf16[4,512,512]{2,1,0:T(8,128)(2,1)S(1)}, bf16[4,512,512]{2,1,0:T(8,128)(2,1)}, u32[]{:S(2)}) copy-start(bf16[4,512,512]{2,1,0:T(8,128)(2,1)} %param.30) | copy-start | bytes 6291460
  71.1 10.7 %all-to-all-start.1 = ((f32[4,1,128]{2,1,0:T(1,128)}), f32[4,1,128]{2,1,0:T(1,128)S(1)}, u32[]{:S(2)}, u32[]{:S(2)}) async-start(f32[4,1,128]{2,1,0:T(1,128)} %reshape.242), calls=%async_computation.1 | async-start | bytes 4096 | tf_op jit(solution)/shard_map/all_to_all | solution.py:166
  81.7 9.2 %all-to-all-start = ((f32[1,64,512]{2,0,1:T(1,128)}), f32[1,64,512]{2,0,1:T(1,128)S(1)}, u32[]{:S(2)}, u32[]{:S(2)}) async-start(f32[1,64,512]{2,0,1:T(1,128)} %broadcast_in_dim_reshape_reshape.4), calls=%async_computation | async-start | bytes 262144 | tf_op jit(solution)/shard_map/all_to_all | solution.py:168
Sparse Core Ops, SparseCore 0:
  11.0 39.9 all-reduce.2
